TPU v7x, 32 devices: a whole 2x2x4 slice. The times are simulated.
32 devices in a mesh: sp: 16 (over z, y, x), tp: 2 (over core).
Axes of the slice: x: 2, y: 2, z: 4, core: 2. Of those that a mesh axis runs over, the one named last changes fastest.
Arguments:
- tokens: bfloat16 [6144, 2048], P(('sp', 'tp')), may hold values from -6 to 6
- norm_gain: float32 [2048], replicated, may hold values from 0.1 to 1.9
- w_query: bfloat16 [2048, 1024], P(None, 'tp'), may hold values from -0.125 to 0.125
- w_key: bfloat16 [2048, 1024], P(None, 'tp'), may hold values from -0.125 to 0.125
- w_value: bfloat16 [2048, 2048], P(None, 'tp'), may hold values from -0.125 to 0.125
- w_ogate: bfloat16 [2048, 2048], P(None, 'tp'), may hold values from -0.125 to 0.125
- w_igate: bfloat16 [2048, 8], replicated, may hold values from -0.125 to 0.125
- w_fgate: bfloat16 [2048, 8], replicated, may hold values from -0.125 to 0.125
- conv_query: bfloat16 [4, 1024], replicated, may hold values from -3 to 3
- conv_key: bfloat16 [4, 1024], replicated, may hold values from -3 to 3
- gate_offset: float32 [2, 48, 8], P(None, 'sp', 'tp'), may hold values from -60 to 140, as said below
- head_gain: float32 [2048], replicated, may hold values from 0.1 to 1.9
- w_out: bfloat16 [2048, 2048], P('tp'), may hold values from -0.125 to 0.125
Outputs:
- mixed: bfloat16 [6144, 2048], P(('sp', 'tp'))
Inputs may be any that keep to these rules, and one draw needn't show every extreme that they name: `gate_offset`: row 0 is added to the input gate's pre-activation and row 1 to the forget gate's; each entry holds for one block of 128 positions and one head.
All inputs are finite; a program needn't handle non-finite values.
Results may differ from a plain program's by a relative error of at most 0.011.
Values may be sent and summed in bfloat16 or wider, within the bound.
A program may use at most 128 MiB of HBM per device.

v0:
```python
import jax
import jax.numpy as jnp
from jax import lax
from jax.sharding import PartitionSpec as P

SPAN = 128


EPS = 1e-06
EMPTY_LEVEL = -1e30
HIGHEST = lax.Precision.HIGHEST


def prefix(part, axis, combine, identity):
    place = lax.axis_index(axis)
    gathered = jax.tree.map(lambda a: lax.all_gather(a, axis), part)
    state = jax.tree.map(lambda a, e: jnp.zeros_like(a) + jnp.asarray(e, a.dtype), part, identity)

    def one(turn, state):
        return combine(
            state, jax.tree.map(lambda a: lax.dynamic_index_in_dim(a, turn, 0, False), gathered)
        )

    return lax.fori_loop(0, place, one, state)


def passed_along(shard, axis, by):
    size = lax.axis_size(axis)
    pairs = [(i, i + by) for i in range(size) if 0 <= i + by < size]
    return lax.ppermute(shard, axis, pairs)


def normalize_rows(values, gain_vec):
    widened = values.astype(jnp.float32)
    scaled = widened * lax.rsqrt(jnp.mean(widened * widened, axis=-1, keepdims=True) + EPS)
    return (scaled * gain_vec).astype(jnp.bfloat16)


def causal_mix(values, leading, weight):
    tap_count = weight.shape[0]
    seq_len = values.shape[0]
    padded = jnp.concatenate([leading, values], axis=0).astype(jnp.float32)
    mixed_sum = jnp.zeros((seq_len, values.shape[1]), jnp.float32)
    for tap_index in range(tap_count):
        mixed_sum = (
            mixed_sum
            + weight[tap_index].astype(jnp.float32) * padded[tap_index : tap_index + seq_len]
        )
    return mixed_sum


def block_read(carried, cumulative, gate_rows, query_blk, key_blk, value_blk):
    states, norm_vec, levels = carried
    span_len = cumulative.shape[1]
    causal = jnp.tril(jnp.ones((span_len, span_len), dtype=bool))
    log_weight = jnp.where(
        causal[None],
        cumulative[:, :, None] - cumulative[:, None, :] + gate_rows[:, None, :],
        -jnp.inf,
    )
    carried_log = cumulative + levels[:, None]
    running_top = jnp.maximum(carried_log, jnp.max(log_weight, axis=-1))
    inner_weight = jnp.exp(log_weight - running_top[:, :, None])
    carried_scale = jnp.exp(carried_log - running_top)
    scores = (
        jnp.einsum("thd,shd->hts", query_blk, key_blk, preferred_element_type=jnp.float32)
        * inner_weight
    )
    query_wide = query_blk.astype(jnp.float32)
    numerator = carried_scale[:, :, None] * jnp.einsum(
        "thd,hde->hte", query_wide, states, precision=HIGHEST
    )
    numerator = numerator + jnp.einsum(
        "hts,she->hte", scores.astype(jnp.bfloat16), value_blk, preferred_element_type=jnp.float32
    )
    denominator = carried_scale * jnp.einsum(
        "thd,hd->ht", query_wide, norm_vec, precision=HIGHEST
    ) + jnp.sum(scores, axis=-1)
    return (numerator, denominator, running_top)


def block_write(carried, cumulative, gate_rows, key_blk, value_blk):
    states, norm_vec, levels = carried
    last_log = cumulative[:, -1]
    write_log = last_log[:, None] - cumulative + gate_rows
    new_levels = jnp.maximum(last_log + levels, jnp.max(write_log, axis=-1))
    decay_scale = jnp.exp(last_log + levels - new_levels)
    write_weight = jnp.exp(write_log - new_levels[:, None])
    weighted = write_weight.T[:, :, None] * key_blk.astype(jnp.float32)
    new_states = decay_scale[:, None, None] * states + jnp.einsum(
        "shd,she->hde", weighted.astype(jnp.bfloat16), value_blk, preferred_element_type=jnp.float32
    )
    new_norm = decay_scale[:, None] * norm_vec + jnp.sum(weighted, axis=0)
    return (new_states, new_norm, new_levels)


def read_write(carried, inputs):
    query_blk, key_blk, value_blk, gate_blk, forget_blk = inputs
    cumulative = jnp.cumsum(forget_blk, axis=0).T
    gate_rows = gate_blk.T
    outputs = block_read(carried, cumulative, gate_rows, query_blk, key_blk, value_blk)
    return (block_write(carried, cumulative, gate_rows, key_blk, value_blk), outputs)


def join_states(earlier_part, later_part):
    forget_one, states_one, norm_one, level_one = earlier_part
    forget_two, states_two, norm_two, level_two = later_part
    shifted = level_one + forget_two
    new_level = jnp.maximum(shifted, level_two)
    scale_one = jnp.exp(shifted - new_level)
    scale_two = jnp.exp(level_two - new_level)
    new_states = scale_one[:, None, None] * states_one + scale_two[:, None, None] * states_two
    new_norm = scale_one[:, None] * norm_one + scale_two[:, None] * norm_two
    return (forget_one + forget_two, new_states, new_norm, new_level)


def pass_state(summary, blank_state):
    return prefix(
        (summary[0], summary[1], summary[2], summary[3]),
        "sp",
        join_states,
        (jnp.zeros_like(summary[0]), blank_state[0], blank_state[1], blank_state[2]),
    )


def unblock(block_parts, seq_len):
    numerator, denominator, running_top = block_parts
    local_heads = numerator.shape[1]
    numerator = jnp.transpose(numerator, (0, 2, 1, 3)).reshape(
        seq_len, local_heads, numerator.shape[3]
    )
    denominator = jnp.transpose(denominator, (0, 2, 1)).reshape(seq_len, local_heads)
    running_top = jnp.transpose(running_top, (0, 2, 1)).reshape(seq_len, local_heads)
    return (numerator, denominator, running_top)


def body(
    tokens,
    norm_gain,
    w_query,
    w_key,
    w_value,
    w_ogate,
    w_igate,
    w_fgate,
    conv_query,
    conv_key,
    gate_offset,
    head_gain,
    w_out,
):
    normed = normalize_rows(tokens, norm_gain)
    gathered = lax.all_gather(normed, "tp", axis=0, tiled=True)
    seq_len = gathered.shape[0]
    local_heads = gate_offset.shape[2]
    key_dim = w_query.shape[1] // local_heads
    value_dim = w_value.shape[1] // local_heads
    head_first = lax.axis_index("tp") * local_heads
    query_pre = jnp.dot(gathered, w_query, preferred_element_type=jnp.float32).astype(jnp.bfloat16)
    key_pre = jnp.dot(gathered, w_key, preferred_element_type=jnp.float32).astype(jnp.bfloat16)
    value_pre = jnp.dot(gathered, w_value, preferred_element_type=jnp.float32).astype(jnp.bfloat16)
    ogate_pre = jnp.dot(gathered, w_ogate, preferred_element_type=jnp.float32).astype(jnp.bfloat16)
    input_cols = lax.dynamic_slice_in_dim(w_igate, head_first, local_heads, 1)
    forget_cols = lax.dynamic_slice_in_dim(w_fgate, head_first, local_heads, 1)
    input_pre = jnp.dot(gathered, input_cols, preferred_element_type=jnp.float32)
    forget_pre = jnp.dot(gathered, forget_cols, preferred_element_type=jnp.float32)
    input_gate = input_pre + jnp.repeat(gate_offset[0], SPAN, axis=0)
    log_forget = jax.nn.log_sigmoid(forget_pre + jnp.repeat(gate_offset[1], SPAN, axis=0))
    tap_count = conv_query.shape[0]
    tail_rows = jnp.stack(
        [query_pre[seq_len - tap_count + 1 :], key_pre[seq_len - tap_count + 1 :]]
    )
    before = passed_along(tail_rows, "sp", 1)
    query_taps = lax.dynamic_slice_in_dim(
        conv_query, head_first * key_dim, local_heads * key_dim, 1
    )
    key_taps = lax.dynamic_slice_in_dim(conv_key, head_first * key_dim, local_heads * key_dim, 1)
    query_rows = (
        jax.nn.silu(causal_mix(query_pre, before[0], query_taps))
        .astype(jnp.bfloat16)
        .reshape(seq_len, local_heads, key_dim)
    )
    key_rows = (
        (jax.nn.silu(causal_mix(key_pre, before[1], key_taps)) * key_dim ** (-0.5))
        .astype(jnp.bfloat16)
        .reshape(seq_len, local_heads, key_dim)
    )
    value_rows = value_pre.reshape(seq_len, local_heads, value_dim)
    blocks = seq_len // SPAN
    blocked = (
        query_rows.reshape(blocks, SPAN, local_heads, key_dim),
        key_rows.reshape(blocks, SPAN, local_heads, key_dim),
        value_rows.reshape(blocks, SPAN, local_heads, value_dim),
        input_gate.reshape(blocks, SPAN, local_heads),
        log_forget.reshape(blocks, SPAN, local_heads),
    )
    blank_state = (
        jnp.zeros((local_heads, key_dim, value_dim), jnp.float32),
        jnp.zeros((local_heads, key_dim), jnp.float32),
        jnp.full((local_heads,), EMPTY_LEVEL, jnp.float32),
    )
    end_state, block_parts = lax.scan(read_write, blank_state, blocked)
    cumulative = jnp.cumsum(log_forget, axis=0)
    incoming = pass_state((cumulative[-1],) + end_state, blank_state)
    numerator, denominator, running_top = unblock(block_parts, seq_len)
    carried_log = cumulative + incoming[3][None, :]
    top_all = jnp.maximum(running_top, carried_log)
    own_scale = jnp.exp(running_top - top_all)
    carried_scale = jnp.exp(carried_log - top_all)
    query_wide = query_rows.astype(jnp.float32)
    from_state = jnp.einsum("thd,hde->the", query_wide, incoming[1], precision=HIGHEST)
    from_norm = jnp.einsum("thd,hd->th", query_wide, incoming[2], precision=HIGHEST)
    numerator = own_scale[:, :, None] * numerator + carried_scale[:, :, None] * from_state
    denominator = own_scale * denominator + carried_scale * from_norm
    cell_out = numerator / jnp.maximum(jnp.abs(denominator), jnp.exp(-top_all))[:, :, None]
    cell_out = cell_out * lax.rsqrt(jnp.mean(cell_out * cell_out, axis=-1, keepdims=True) + EPS)
    gain_local = lax.dynamic_slice_in_dim(
        head_gain, head_first * value_dim, local_heads * value_dim, 0
    )
    hidden = (
        cell_out.reshape(seq_len, local_heads * value_dim)
        * gain_local
        * jax.nn.sigmoid(ogate_pre.astype(jnp.float32))
    )
    hidden = hidden.astype(jnp.bfloat16)
    return lax.psum_scatter(
        jnp.dot(hidden, w_out, preferred_element_type=jnp.float32).astype(jnp.bfloat16),
        "tp",
        scatter_dimension=0,
        tiled=True,
    )


def solution(mesh):
    in_specs = (
        P(("sp", "tp"), None),
        P(),
        P(None, "tp"),
        P(None, "tp"),
        P(None, "tp"),
        P(None, "tp"),
        P(),
        P(),
        P(),
        P(),
        P(None, "sp", "tp"),
        P(),
        P("tp", None),
    )
    out_specs = P(("sp", "tp"), None)
    return jax.shard_map(body, mesh=mesh, in_specs=in_specs, out_specs=out_specs, check_vma=False)
```

profile of v0, /device:TPU:15, one launch (start us, length us, event | category | flops | bytes accessed | tf_op | source)
XLA Modules:
  0.0 242.1 jit_solution(1840042009361809394)
XLA Ops:
  6.6 1.5 fusion.22
  8.1 2.3 fusion.24
  10.7 11.5 %all-gather.8.cloned.1.call-done = bf16[384,2048]{1,0:T(8,128)(2,1)} async-done(((bf16[192,2048]{1,0:T(8,128)(2,1)}), bf16[384,2048]{1,0:T(8,128)(2,1)}) %all-gather.8.cloned.1.call-update) | async-done | bytes 1572880 | tf_op jit(solution)/shard_map/all_gather | solution.py:153
  22.2 2.5 %convolution_convert_fusion.3 = bf16[384,512]{1,0:T(8,128)(2,1)S(1)} fusion(bf16[384,2048]{1,0:T(8,128)(2,1)} %all-gather.8.cloned.1.call-done, bf16[2048,512]{1,0:T(8,128)(2,1)S(1)} %copy-done), kind=kOutput, calls=%fused_computation.66 | convolution fusion | flops 805502976 | bytes 4063232 | tf_op jit(solution)/shard_map/dot_general | solution.py:160
  24.7 1.0 convolution_convert_fusion.4
  25.8 0.7 copy-done.4
  26.5 3.1 %collective-permute-start = (bf16[2,3,512]{2,1,0:T(4,128)(2,1)S(1)}, bf16[2,3,512]{2,1,0:T(4,128)(2,1)S(1)}, u32[]{:S(2)}, u32[]{:S(2)}) collective-permute-start(bf16[2,3,512]{2,1,0:T(4,128)(2,1)S(1)} %pad_maximum_fusion), channel_id=1, source_target_pairs={{0,2},{2,4},{4,6},{6,8},{8,10},{10,12},{12,14},{14,16},{16,18},{18... | collective-permute-start | bytes 18440 | tf_op jit(solution)/shard_map/ppermute | solution.py:30
  29.6 2.7 %convolution_convert_fusion.2 = bf16[384,1024]{1,0:T(8,128)(2,1)} fusion(bf16[384,2048]{1,0:T(8,128)(2,1)S(1)} %copy-done.2, bf16[2048,1024]{1,0:T(8,128)(2,1)S(1)} %copy-done.15), kind=kOutput, calls=%fused_computation.65 | convolution fusion | flops 1611005952 | bytes 6553600 | tf_op jit(solution)/shard_map/dot_general | solution.py:161
  32.3 0.5 fusion.37
  33.1 0.5 fusion.27
  33.6 2.0 reshape_reshape.10
  35.6 1.1 maximum_convert_fusion.1
  36.7 1.2 multiply_convert_fusion.1
  37.9 1.8 reshape_reshape.11
  39.8 1.1 maximum_convert_fusion
  40.9 1.3 multiply_convert_fusion.2
  42.1 1.8 reshape_reshape.9
  44.0 23.2 %while.38 = (s32[]{:T(128)}, f32[4,128,256]{2,1,0:T(8,128)S(1)}, f32[4,128]{1,0:T(4,128)}, f32[4]{0:T(128)}, f32[3,4,128,256]{3,2,0,1:T(8,128)}, /*index=5*/f32[...) while((s32[]{:T(128)}, f32[4,128,256]{2,1,0:T(8,128)S(1)}, ...), condition=%wide.region_7.8_spmd.clone, body=%wide.region_1.7_spmd.clone.sunk | while | flops 287987200 | bytes 5902382 | solution.py:202
  44.8 1.1 constant_dynamic-slice_fusion.12
  46.1 0.6 multiply_add_fusion.2
  47.3 0.7 bitcast_dynamic-update-slice_fusion.4
  48.2 0.7 bitcast_dynamic-update-slice_fusion.5
  48.8 0.4 convolution_multiply_fusion.3
  49.4 1.1 fusion.95
  50.5 0.4 convolution_add_fusion.5
  51.6 0.6 fusion.89
  52.4 1.1 constant_dynamic-slice_fusion.12
  53.6 1.3 multiply_add_fusion.2
  55.4 0.6 bitcast_dynamic-update-slice_fusion.4
  56.3 0.6 bitcast_dynamic-update-slice_fusion.5
  56.9 0.4 convolution_multiply_fusion.3
  57.5 1.1 fusion.95
  58.6 0.4 convolution_add_fusion.5
  59.7 0.6 fusion.89
  60.5 1.1 constant_dynamic-slice_fusion.12
  61.7 1.3 multiply_add_fusion.2
  63.5 0.7 bitcast_dynamic-update-slice_fusion.4
  64.4 0.7 bitcast_dynamic-update-slice_fusion.5
  65.1 0.4 convolution_multiply_fusion.3
  65.7 1.1 fusion.95
  66.7 0.4 convolution_add_fusion.5
  67.2 0.8 copy-done.1
  68.1 1.2 dynamic-slice
  69.9 1.2 reduce-window.6
  71.7 21.6 %all-gather.3 = f32[16,1,4]{2,1,0:T(1,128)S(1)} all-gather(f32[1,1,4]{2,1,0:T(1,128)S(1)} %bitcast.263), channel_id=1, replica_groups=mesh['sp'=16,'tp'=2] {'sp'}, dimensions={0}, use_global_device_ids=true | all-gather | bytes 272 | tf_op jit(solution)/shard_map/all_gather | solution.py:16
  93.3 1.2 copy.161
  94.5 3.1 %copy.136 = f32[384,4,256]{0,2,1:T(8,128)} copy(f32[384,4,256]{2,0,1:T(8,128)} %bitcast.242) | data formatting | bytes 3145728 | tf_op jit(solution)/shard_map/reshape | solution.py:129
  97.8 31.7 %all-reduce = f32[64]{0:T(128)S(1)} all-reduce(f32[64]{0:T(128)S(1)} %dynamic-update-slice), channel_id=2, replica_groups=mesh['sp'=16,'tp'=2] {'sp'}, use_global_device_ids=true, to_apply=%add | all-reduce | flops 64 | bytes 512
  129.6 32.7 %all-gather.4 = f32[16,4,128]{2,1,0:T(4,128)S(1)} all-gather(f32[1,4,128]{2,1,0:T(4,128)S(1)} %bitcast.249), channel_id=4, replica_groups=mesh['sp'=16,'tp'=2] {'sp'}, dimensions={0}, use_global_device_ids=true | all-gather | bytes 34816 | tf_op jit(solution)/shard_map/all_gather | solution.py:16
  162.3 16.4 %all-gather.10.cloned.1.call-done = f32[64,128,256]{2,1,0:T(8,128)} async-done(((f32[4,128,256]{2,1,0:T(8,128)}), f32[64,128,256]{2,1,0:T(8,128)}) %all-gather.10.cloned.1.call-update) | async-done | bytes 8388624 | tf_op jit(solution)/shard_map/all_gather | solution.py:16
  178.7 10.2 %while.37 = (s32[]{:T(128)}, f32[4,128,256]{2,1,0:T(8,128)S(1)}, f32[4,128]{1,0:T(4,128)S(1)}, f32[4]{0:T(128)S(1)}, s32[]{:T(128)}, /*index=5*/f32[16,4]{1,0:T(...) while((s32[]{:T(128)}, f32[4,128,256]{2,1,0:T(8,128)S(1)}, ...), condition=%wide.region_11.12_spmd, body=%wide.region_10.11_spmd.sunk | while | flops 394773 | bytes 1579367 | solution.py:24
  178.8 1.3 fusion.83
  180.2 1.3 fusion.83
  181.7 1.3 fusion.83
  183.1 1.3 fusion.83
  184.5 1.3 fusion.83
  186.0 1.3 fusion.83
  187.4 1.3 fusion.83
  188.9 0.3 fusion.52
  189.3 2.5 %multiply_reduce_fusion = (f32[384,4]{0,1:T(4,128)S(1)}, f32[384,4,256]{0,2,1:T(8,128)S(1)}) fusion(f32[384,4]{0,1:T(4,128)S(1)} %get-tuple-element.381, f32[4,128,256]{2,1,0:T(8,128)S(1)} %get-tuple-element.152, bf16[384,4,128]{0,2,1:T(8,128)(2,1)S(1)} %bitcast.244, f32[384,4]{0,1:T(4,128)S(1)} %get-tuple-element.382, f32[384,4,256]{0,2,1:T(8,128)} %copy.136, ...), kind=kOutput, calls=%fused_computation.63 | convolution fusion | flops 606337536 | bytes 4087808 | tf_op jit(solution)/shard_map/thd,hde->the/dot_general | solution.py:211
  191.9 1.3 broadcast_multiply_fusion
  193.1 3.0 %copy.139 = f32[384,1024]{1,0:T(8,128)} copy(f32[384,1024]{0,1:T(8,128)} %bitcast.238) | data formatting | bytes 3145728 | tf_op jit(solution)/shard_map/reshape | solution.py:221
  196.2 9.0 %convolution_convert_fusion = bf16[384,2048]{1,0:T(8,128)(2,1)} fusion(bf16[1024,2048]{1,0:T(8,128)(2,1)} %param.29, f32[384,1024]{1,0:T(8,128)} %copy.139, bf16[384,2048]{1,0:T(8,128)(2,1)} %all-gather.8.cloned.1.call-done, bf16[2048,1024]{1,0:T(8,128)(2,1)} %param.22, f32[1024]{0:T(1024)S(1)} %dynamic-slice-done), kind=kOutput, calls=%fused_computation.53 | convolution fusion | flops 3225157632 | bytes 13111296 | tf_op jit(solution)/shard_map/dot_general | solution.py:227
  205.2 30.3 %reduce-scatter.2.cloned.1.call-done = bf16[192,2048]{1,0:T(8,128)(2,1)} async-done(((bf16[384,2048]{1,0:T(8,128)(2,1)}), bf16[192,2048]{1,0:T(8,128)(2,1)}) %reduce-scatter.2.cloned.1.call-update) | async-done | bytes 786448 | tf_op jit(solution)/shard_map/reduce_scatter | solution.py:226
  (136 shorter events, 8.0 us)
Async XLA Ops:
  6.5 15.6 %copy-start = (bf16[2048,512]{1,0:T(8,128)(2,1)S(1)}, bf16[2048,512]{1,0:T(8,128)(2,1)}, u32[]{:S(2)}) copy-start(bf16[2048,512]{1,0:T(8,128)(2,1)} %param.20) | copy-start | bytes 6291460
  6.5 4.0 %copy-start.10 = (bf16[4,1024]{1,0:T(4,128)(2,1)S(1)}, bf16[4,1024]{1,0:T(4,128)(2,1)}, u32[]{:S(2)}) copy-start(bf16[4,1024]{1,0:T(4,128)(2,1)} %param.25) | copy-start | bytes 24580
  6.5 4.0 %copy-start.11 = (bf16[4,1024]{1,0:T(4,128)(2,1)S(1)}, bf16[4,1024]{1,0:T(4,128)(2,1)}, u32[]{:S(2)}) copy-start(bf16[4,1024]{1,0:T(4,128)(2,1)} %param.26) | copy-start | bytes 24580
  6.5 4.1 %copy-start.14 = (f32[2,3,4]{2,0,1:T(2,128)S(1)}, f32[2,3,4]{2,0,1:T(2,128)}, u32[]{:S(2)}) copy-start(f32[2,3,4]{2,0,1:T(2,128)} %param.27) | copy-start | bytes 292
  6.5 15.6 %all-gather.8.cloned.1.call-start = ((), (), s32[]{:S(2)}) async-start(), calls=%async_computation.1 | async-start | bytes 2359296 | tf_op jit(solution)/shard_map/all_gather | solution.py:153
  10.4 168.2 %all-gather.10.cloned.1.call-start = ((), (), s32[]{:S(2)}) async-start(), calls=%async_computation.3 | async-start | bytes 8912896 | tf_op jit(solution)/shard_map/all_gather | solution.py:16
  22.2 2.5 %copy-start.2 = (bf16[384,2048]{1,0:T(8,128)(2,1)S(1)}, bf16[384,2048]{1,0:T(8,128)(2,1)}, u32[]{:S(2)}) copy-start(bf16[384,2048]{1,0:T(8,128)(2,1)} %all-gather.8.cloned.1.call-done) | copy-start | bytes 4718596
  22.2 2.5 %copy-start.16 = (bf16[2048,512]{1,0:T(8,128)(2,1)S(1)}, bf16[2048,512]{1,0:T(8,128)(2,1)}, u32[]{:S(2)}) copy-start(bf16[2048,512]{1,0:T(8,128)(2,1)} %param.19) | copy-start | bytes 6291460
  24.7 1.0 copy-start.3
  24.7 4.9 %copy-start.15 = (bf16[2048,1024]{1,0:T(8,128)(2,1)S(1)}, bf16[2048,1024]{1,0:T(8,128)(2,1)}, u32[]{:S(2)}) copy-start(bf16[2048,1024]{1,0:T(8,128)(2,1)} %param.21) | copy-start | bytes 12582916
  25.7 0.7 copy-start.4
  26.5 5.8 %copy-start.8 = (bf16[2048,8]{0,1:T(8,128)(2,1)S(1)}, bf16[2048,8]{0,1:T(8,128)(2,1)}, u32[]{:S(2)}) copy-start(bf16[2048,8]{0,1:T(8,128)(2,1)} %param.24) | copy-start | bytes 98308
  26.5 9.1 %collective-permute-start = (bf16[2,3,512]{2,1,0:T(4,128)(2,1)S(1)}, bf16[2,3,512]{2,1,0:T(4,128)(2,1)S(1)}, u32[]{:S(2)}, u32[]{:S(2)}) collective-permute-start(bf16[2,3,512]{2,1,0:T(4,128)(2,1)S(1)} %pad_maximum_fusion), channel_id=1, source_target_pairs={{0,2},{2,4},{4,6},{6,8},{8,10},{10,12},{12,14},{14,16},{16,18},{18... | collective-permute-start | bytes 18440 | tf_op jit(solution)/shard_map/ppermute | solution.py:30
  32.3 0.8 copy-start.9
  44.8 4.6 %copy-start.6 = (f32[4]{0:T(128)}, f32[4]{0:T(128)S(1)}, u32[]{:S(2)}) copy-start(f32[4]{0:T(128)S(1)} %get-tuple-element.605) | copy-start | bytes 52 | tf_op jit(solution)/shard_map/while
  52.3 5.2 %copy-start.6 = (f32[4]{0:T(128)}, f32[4]{0:T(128)S(1)}, u32[]{:S(2)}) copy-start(f32[4]{0:T(128)S(1)} %get-tuple-element.605) | copy-start | bytes 52 | tf_op jit(solution)/shard_map/while
  60.4 5.3 %copy-start.6 = (f32[4]{0:T(128)}, f32[4]{0:T(128)S(1)}, u32[]{:S(2)}) copy-start(f32[4]{0:T(128)S(1)} %get-tuple-element.605) | copy-start | bytes 52 | tf_op jit(solution)/shard_map/while
  67.2 0.8 copy-start.1
  68.0 167.6 %reduce-scatter.2.cloned.1.call-start = ((), (), s32[]{:S(2)}) async-start(), calls=%async_computation.2 | async-start | bytes 2359296 | tf_op jit(solution)/shard_map/reduce_scatter | solution.py:226
  94.5 3.1 %copy-start.7 = (f32[4]{0:T(128)S(1)}, f32[4]{0:T(128)}, u32[]{:S(2)}) copy-start(f32[4]{0:T(128)} %get-tuple-element.147) | copy-start | bytes 52
  94.5 35.1 %copy-start.5 = (f32[4,128]{1,0:T(4,128)S(1)}, f32[4,128]{1,0:T(4,128)}, u32[]{:S(2)}) copy-start(f32[4,128]{1,0:T(4,128)} %get-tuple-element.149) | copy-start | bytes 6148
  178.7 10.5 %copy-start.12 = (f32[3,4,128]{2,1,0:T(4,128)S(1)}, f32[3,4,128]{2,1,0:T(4,128)}, u32[]{:S(2)}) copy-start(f32[3,4,128]{2,1,0:T(4,128)} %get-tuple-element.153) | copy-start | bytes 18436
  178.7 10.5 %copy-start.13 = (f32[3,4,128]{2,1,0:T(4,128)S(1)}, f32[3,4,128]{2,1,0:T(4,128)}, u32[]{:S(2)}) copy-start(f32[3,4,128]{2,1,0:T(4,128)} %get-tuple-element.146) | copy-start | bytes 18436
  193.1 3.1 %dynamic-slice-start = ((f32[2048]{0:T(1024)}, s32[]{:T(128)}), f32[1024]{0:T(1024)S(1)}, s32[]{:S(2)}) async-start(f32[2048]{0:T(1024)} %param.28, s32[]{:T(128)} %select_n.35), calls=%async_computation.4 | async-start | bytes 8704 | tf_op jit(solution)/shard_map/dynamic_slice | solution.py:217
Sparse Core Ops, SparseCore 0:
  10.5 11.6 all-gather.7
  68.1 110.4 all-gather.9
  205.4 30.1 reduce-scatter.1
where the time goes:
time: 244 us; the launch traced here: 242 us
  blocking collectives  86 us (35%)
  waiting for transfers between devices  58.2 us (24%)
  other arithmetic  32.4 us (13%)
  matrix products  26.4 us (11%)
  local copies, waits for them, and re-layouts  21.3 us (9%)
  between operations  14.1 us (6%)
  starting transfers between devices  3.22 us (1%)
    all_gather x2, blocking collectives, prefix(): gathered = jax.tree.map(lambda a: lax.all_gather(a, axis), part)  54.3 us
    unnamed x1, blocking collectives  31.7 us
    reduce_scatter x1, waiting for transfers between devices, body(): lax.psum_scatter(jnp.dot(hidden, w_out, preferred_element_type=jnp.float3...  30.3 us
    all_gather x1, waiting for transfers between devices, prefix(): gathered = jax.tree.map(lambda a: lax.all_gather(a, axis), part)  16.4 us
    all_gather x1, waiting for transfers between devices, body(): gathered = lax.all_gather(normed, 'tp', axis=0, tiled=True)  11.5 us
    add x7, other arithmetic, join_states(): scale_one[:, None, None] * states_one  9.18 us
    dot_general x1, matrix products, body(): jnp.dot(hidden, w_out, preferred_element_type=jnp.float32)  9.03 us
  transfers between devices with their start and end apart: 4, of which 3 were waited for; matrix products, arithmetic and copies ran while one was open for 6% of the time, Pallas kernels for 0%

commit v1 on v0

v1 whole, which is shorter than its diff:
```python
import functools

import jax
import jax.numpy as jnp
from jax import lax
from jax.experimental import pallas as pl
from jax.experimental.pallas import tpu as pltpu
from jax.sharding import PartitionSpec as P

SPAN = 128
HALO = 16
EPS = 1e-06
EMPTY_LEVEL = -1e30
HIGHEST = lax.Precision.HIGHEST
MESH = pl.DeviceIdType.MESH
F32, BF16 = jnp.float32, jnp.bfloat16


def normalize(values, gain):
    widened = values.astype(F32)
    scaled = widened * lax.rsqrt(jnp.mean(widened * widened, axis=-1, keepdims=True) + EPS)
    return (scaled * gain).astype(BF16)


def dot_t(a, b):
    return lax.dot_general(a, b, (((1,), (1,)), ((), ())), preferred_element_type=F32)


def dot_tl(a, b):
    return lax.dot_general(a, b, (((0,), (0,)), ((), ())), preferred_element_type=F32)


def kernel(
    sp,
    tp,
    tokens_hbm,
    gain_ref,
    wq_hbm,
    wk_hbm,
    wv_hbm,
    wo_hbm,
    wi_ref,
    wf_ref,
    cq_ref,
    ck_ref,
    offset_ref,
    hgain_ref,
    wout_hbm,
    out_ref,
    ext,
    normed,
    wq,
    wk,
    wv,
    wo,
    wout,
    pre,
    key,
    query,
    value,
    ogate,
    numer,
    cols,
    hidden,
    sbuf,
    rbuf,
    meta,
    mbuf,
    pbuf,
    gbuf,
    sharesend,
    sharerecv,
    w_sem,
    t_sem,
    tsend_sem,
    trecv_sem,
    hsend_sem,
    hrecv_sem,
    psend_sem,
    precv_sem,
    msend_sem,
    mrecv_sem,
    gsend_sem,
    grecv_sem,
    osend_sem,
    orecv_sem,
):
    me = lax.axis_index("sp")
    core = lax.axis_index("tp")
    rows, model = tokens_hbm.shape
    seq_len = rows * tp
    blocks = seq_len // SPAN
    heads = offset_ref.shape[2]
    dqk = wq.shape[1] // heads
    dv = wv.shape[1] // heads
    piece_rows = sbuf.shape[1]
    head_first = core * heads

    own_rows = pl.ds(pl.multiple_of(HALO + core * rows, 16), rows)
    own_copy = pltpu.make_async_copy(tokens_hbm, ext.at[own_rows], t_sem)
    own_copy.start()
    streams = {}
    at = 0
    for name, hbm, vm in (
        ("v", wv_hbm, wv),
        ("k", wk_hbm, wk),
        ("q", wq_hbm, wq),
        ("o", wo_hbm, wo),
        ("out", wout_hbm, wout),
    ):
        streams[name] = []
        for c in range(0, hbm.shape[1], 512):
            cp = pltpu.make_async_copy(
                hbm.at[:, pl.ds(c, 512)], vm.at[:, pl.ds(c, 512)], w_sem.at[at]
            )
            cp.start()
            streams[name].append(cp)
            at += 1

    barrier = pltpu.get_barrier_semaphore()

    def greet(d, c):
        pl.semaphore_signal(
            barrier, inc=1, device_id=(lax.rem(me + d, sp), core), device_id_type=MESH
        )
        return c

    lax.fori_loop(1, sp, greet, 0)
    for d in range(1, tp):
        pl.semaphore_signal(
            barrier, inc=1, device_id=(me, lax.rem(core + d, tp)), device_id_type=MESH
        )
    pl.semaphore_wait(barrier, sp - 1 + tp - 1)

    token_sends = []
    for d in range(1, tp):
        cp = pltpu.make_async_remote_copy(
            src_ref=tokens_hbm,
            dst_ref=ext.at[own_rows],
            send_sem=tsend_sem.at[d],
            recv_sem=trecv_sem.at[d],
            device_id=(me, lax.rem(core + d, tp)),
            device_id_type=MESH,
        )
        cp.start()
        token_sends.append(cp)

    own_copy.wait()
    gain = gain_ref[...]
    normed[own_rows, :] = normalize(ext[own_rows, :], gain)
    for d in range(1, tp):
        token_sends[d - 1].wait_send()
        src_core = lax.rem(core + tp - d, tp)
        their = pl.ds(pl.multiple_of(HALO + src_core * rows, 16), rows)
        pltpu.make_async_remote_copy(
            src_ref=tokens_hbm,
            dst_ref=ext.at[their],
            send_sem=tsend_sem.at[d],
            recv_sem=trecv_sem.at[d],
            device_id=(me, src_core),
            device_id_type=MESH,
        ).wait_recv()
    halo = pltpu.make_async_remote_copy(
        src_ref=ext.at[pl.ds(seq_len, HALO)],
        dst_ref=ext.at[pl.ds(0, HALO)],
        send_sem=hsend_sem,
        recv_sem=hrecv_sem,
        device_id=(lax.rem(me + 1, sp), core),
        device_id_type=MESH,
    )

    @pl.when(me < sp - 1)
    def _():
        halo.start()

    for d in range(1, tp):
        src_core = lax.rem(core + tp - d, tp)
        their = pl.ds(pl.multiple_of(HALO + src_core * rows, 16), rows)
        normed[their, :] = normalize(ext[their, :], gain)

    body_rows = pl.ds(HALO, seq_len)

    gates_all = dot_t(
        jnp.concatenate([wi_ref[...], wf_ref[...]], axis=0), normed[body_rows, :]
    )
    total_heads = wi_ref.shape[0]
    in_rows = gates_all[:heads]
    fo_rows = gates_all[total_heads : total_heads + heads]
    for c in range(1, tp):
        in_rows = jnp.where(core == c, gates_all[c * heads : (c + 1) * heads], in_rows)
        fo_rows = jnp.where(
            core == c,
            gates_all[total_heads + c * heads : total_heads + (c + 1) * heads],
            fo_rows,
        )
    head_id = lax.broadcasted_iota(jnp.int32, (heads, SPAN), 0)

    def offsets(kind, b):
        spread = jnp.zeros((heads, SPAN), F32)
        for h in range(heads):
            spread = jnp.where(head_id == h, offset_ref[kind, b, h], spread)
        return spread

    upper = (
        lax.broadcasted_iota(jnp.int32, (SPAN, SPAN), 0)
        <= lax.broadcasted_iota(jnp.int32, (SPAN, SPAN), 1)
    ).astype(F32)
    gate, cum, tot = [], [], []
    for b in range(blocks):
        part = slice(b * SPAN, (b + 1) * SPAN)
        gate.append(in_rows[:, part] + offsets(0, b))
        x = fo_rows[:, part] + offsets(1, b)
        lf = jnp.minimum(x, 0.0) - jnp.log1p(jnp.exp(-jnp.abs(x)))
        lf8 = jnp.concatenate([lf, jnp.zeros((8 - heads, SPAN), F32)], axis=0) if heads < 8 else lf
        c = jnp.dot(lf8, upper, precision=HIGHEST, preferred_element_type=F32)[:heads]
        cum.append(c)
        tot.append(c[:, SPAN - 1 :])
    base = [jnp.zeros((heads, 1), F32)]
    for b in range(blocks):
        base.append(base[-1] + tot[b])
    tail = [None] * blocks
    acc = jnp.zeros((heads, 1), F32)
    for b in reversed(range(blocks)):
        tail[b] = acc
        acc = acc + tot[b]
    wlog = [tail[b] + (tot[b] - cum[b]) + gate[b] for b in range(blocks)]
    level = jnp.max(wlog[0], axis=1, keepdims=True)
    for b in range(1, blocks):
        level = jnp.maximum(level, jnp.max(wlog[b], axis=1, keepdims=True))
    wrows = [jnp.exp(w - level) for w in wlog]
    stacked = [jnp.concatenate([cum[b], wrows[b]], axis=0).T for b in range(blocks)]

    for c, cp in enumerate(streams["v"]):
        cp.wait()
        for n in range(c * 512, c * 512 + 512, 256):
            value[:, n : n + 256] = jnp.dot(
                normed[body_rows, :], wv[:, n : n + 256], preferred_element_type=F32
            ).astype(BF16)

    @pl.when(me < sp - 1)
    def _():
        halo.wait_send()

    @pl.when(me > 0)
    def _():
        halo.wait_recv()

    @pl.when(me == 0)
    def _():
        ext[pl.ds(0, HALO), :] = jnp.zeros((HALO, model), BF16)

    normed[pl.ds(0, HALO), :] = normalize(ext[pl.ds(0, HALO), :], gain)

    def project_mix(stream, w, taps_ref, dest, scale):
        for cp in stream:
            cp.wait()
        width = w.shape[1]
        for n in range(0, width, 256):
            pre[:, n : n + 256] = (
                jnp.dot(normed[...], w[:, n : n + 256], preferred_element_type=F32)
                .astype(BF16)
                .astype(F32)
            )
        taps = taps_ref[:, pl.ds(pl.multiple_of(core * width, 128), width)].astype(F32)
        count = taps.shape[0]
        for n in range(0, width, 128):
            mixed = jnp.zeros((seq_len, 128), F32)
            for j in range(count):
                mixed = (
                    mixed
                    + taps[j : j + 1, n : n + 128]
                    * pre[pl.ds(HALO - count + 1 + j, seq_len), n : n + 128]
                )
            dest[:, n : n + 128] = (mixed * jax.nn.sigmoid(mixed) * scale).astype(BF16)

    project_mix(streams["k"], wk, ck_ref, key, dqk**-0.5)

    for h in range(heads):
        weighted = [
            stacked[b][:, heads + h : heads + h + 1]
            * key[b * SPAN : (b + 1) * SPAN, h * dqk : (h + 1) * dqk].astype(F32)
            for b in range(blocks)
        ]
        norm = jnp.sum(weighted[0], axis=0, keepdims=True)
        for b in range(1, blocks):
            norm = norm + jnp.sum(weighted[b], axis=0, keepdims=True)
        state = dot_tl(
            jnp.concatenate([w.astype(BF16) for w in weighted], axis=0),
            value[:, h * dv : (h + 1) * dv],
        )
        per = dqk // piece_rows
        for p in range(per):
            sbuf[h * per + p] = state[p * piece_rows : (p + 1) * piece_rows].astype(BF16)
        meta[0, h : h + 1, :] = norm
    meta[1] = jnp.broadcast_to(base[blocks], (heads, dqk))
    meta[2] = jnp.broadcast_to(level, (heads, dqk))

    def piece_copy(source, target, d):
        return pltpu.make_async_remote_copy(
            src_ref=sbuf.at[target],
            dst_ref=rbuf.at[source],
            send_sem=psend_sem.at[d],
            recv_sem=precv_sem.at[source],
            device_id=(target, core),
            device_id_type=MESH,
        )

    def meta_copy(source, target, d):
        return pltpu.make_async_remote_copy(
            src_ref=meta,
            dst_ref=mbuf.at[source],
            send_sem=msend_sem.at[d],
            recv_sem=mrecv_sem.at[source],
            device_id=(target, core),
            device_id_type=MESH,
        )

    def prefix_copy(source, target):
        return pltpu.make_async_remote_copy(
            src_ref=pbuf.at[target],
            dst_ref=gbuf.at[source],
            send_sem=gsend_sem.at[target],
            recv_sem=grecv_sem.at[source],
            device_id=(target, core),
            device_id_type=MESH,
        )

    def send_one(d, c):
        target = lax.rem(me + d, sp)
        meta_copy(me, target, d).start()
        piece_copy(me, target, d).start()
        return c

    lax.fori_loop(1, sp, send_one, 0)
    rbuf[me] = sbuf[me]
    mbuf[me] = meta[...]

    project_mix(streams["q"], wq, cq_ref, query, 1.0)

    causal = lax.broadcasted_iota(jnp.int32, (SPAN, SPAN), 0) >= lax.broadcasted_iota(
        jnp.int32, (SPAN, SPAN), 1
    )

    def intra(h):
        for i in range(blocks):
            col = stacked[i][:, h : h + 1]
            logs = []
            top = None
            for j in range(i + 1):
                row = (gate[j][h : h + 1] - cum[j][h : h + 1]) + (
                    base[i][h : h + 1] - base[j][h : h + 1]
                )
                tile = col + row
                if j == i:
                    tile = jnp.where(causal, tile, -jnp.inf)
                logs.append(tile)
                t = jnp.max(tile, axis=1, keepdims=True)
                top = t if top is None else jnp.maximum(top, t)
            q = query[i * SPAN : (i + 1) * SPAN, h * dqk : (h + 1) * dqk]
            den = jnp.zeros((SPAN, 1), F32)
            num = jnp.zeros((SPAN, dv), F32)
            for j in range(i + 1):
                k = key[j * SPAN : (j + 1) * SPAN, h * dqk : (h + 1) * dqk]
                scores = dot_t(q, k) * jnp.exp(logs[j] - top)
                den = den + jnp.sum(scores, axis=1, keepdims=True)
                num = num + jnp.dot(
                    scores.astype(BF16),
                    value[j * SPAN : (j + 1) * SPAN, h * dv : (h + 1) * dv],
                    preferred_element_type=F32,
                )
            numer[i * SPAN : (i + 1) * SPAN, h * dv : (h + 1) * dv] = num
            cols[h, i * SPAN : (i + 1) * SPAN, 0:1] = den
            cols[h, i * SPAN : (i + 1) * SPAN, 1:2] = top

    for h in range(heads):
        intra(h)

    per_head = sp // heads
    my_head = me // per_head
    small_id = lax.broadcasted_iota(jnp.int32, (heads, dqk), 0)

    def pick(x):
        r = jnp.sum(jnp.where(small_id == my_head, x, 0.0), axis=0, keepdims=True)
        return jnp.concatenate([r] * (dv // dqk), axis=1)

    def combine(i, carry):
        lev, nor, piece, lev_in, nor_in = carry
        j = i - 1

        @pl.when(j != me)
        def _():
            meta_copy(j, me, 0).wait_recv()
            piece_copy(j, me, 0).wait_recv()

        shifted = lev + mbuf[j, 1]
        new_lev = jnp.maximum(shifted, mbuf[j, 2])
        one, two = jnp.exp(shifted - new_lev), jnp.exp(mbuf[j, 2] - new_lev)
        nor = one * nor + two * mbuf[j, 0]
        piece = pick(one) * piece + pick(two) * rbuf[j].astype(F32)
        pbuf[i] = piece.astype(BF16)

        @pl.when(i == me)
        def _():
            gbuf[me] = piece.astype(BF16)

        @pl.when(jnp.logical_and(i > 1, j != me))
        def _():
            prefix_copy(me, j).start()

        lev_in = jnp.where(i == me, new_lev, lev_in)
        nor_in = jnp.where(i == me, nor, nor_in)
        return new_lev, nor, piece, lev_in, nor_in

    empty = jnp.full((heads, dqk), EMPTY_LEVEL, F32)
    none = jnp.zeros((heads, dqk), F32)
    _, _, _, lev_in, nor_in = lax.fori_loop(
        1, sp, combine, (empty, none, jnp.zeros((piece_rows, dv), F32), empty, none)
    )

    @pl.when(me != sp - 1)
    def _():
        prefix_copy(me, sp - 1).start()

    @pl.when(me != sp - 1)
    def _():
        meta_copy(sp - 1, me, 0).wait_recv()
        piece_copy(sp - 1, me, 0).wait_recv()

    for c, cp in enumerate(streams["o"]):
        cp.wait()
        for n in range(c * 512, c * 512 + 512, 256):
            ogate[:, n : n + 256] = jnp.dot(
                normed[body_rows, :], wo[:, n : n + 256], preferred_element_type=F32
            ).astype(BF16)

    @pl.when(me == 0)
    def _():
        gbuf[...] = jnp.zeros(gbuf.shape, BF16)

    def take(d, c):
        prefix_copy(lax.rem(me + d, sp), me).wait_recv()
        return c

    @pl.when(me > 0)
    def _():
        lax.fori_loop(1, sp, take, 0)

    per = dqk // piece_rows
    for h in range(heads):
        state = jnp.concatenate([gbuf[h * per + p] for p in range(per)], axis=0)
        hgain = hgain_ref[:, pl.ds(pl.multiple_of((head_first + h) * dv, 128), dv)]
        for i in range(blocks):
            part = slice(i * SPAN, (i + 1) * SPAN)
            q = query[part, h * dqk : (h + 1) * dqk]
            carried = (stacked[i][:, h : h + 1] + base[i][h : h + 1]) + lev_in[h : h + 1, 0:1]
            den, own_top = cols[h, part, 0:1], cols[h, part, 1:2]
            top = jnp.maximum(own_top, carried)
            own, old = jnp.exp(own_top - top), jnp.exp(carried - top)
            from_norm = jnp.sum(q.astype(F32) * nor_in[h : h + 1], axis=1, keepdims=True)
            den = own * den + old * from_norm
            num = own * numer[part, h * dv : (h + 1) * dv] + old * jnp.dot(
                q, state, preferred_element_type=F32
            )
            cell = num / jnp.maximum(jnp.abs(den), jnp.exp(-top))
            cell = cell * lax.rsqrt(jnp.mean(cell * cell, axis=-1, keepdims=True) + EPS)
            hidden[part, h * dv : (h + 1) * dv] = (
                cell * hgain * jax.nn.sigmoid(ogate[part, h * dv : (h + 1) * dv].astype(F32))
            ).astype(BF16)

    sends = []
    chunks = len(streams["out"])
    for c, cp in enumerate(streams["out"]):
        cp.wait()
    for d in range(1, tp):
        target = lax.rem(core + d, tp)
        theirs = pl.ds(pl.multiple_of(target * rows, 16), rows)
        for c in range(chunks):
            sharesend[d - 1, c] = jnp.dot(
                hidden[theirs, :], wout[:, c * 512 : (c + 1) * 512], preferred_element_type=F32
            ).astype(BF16)
            cp = pltpu.make_async_remote_copy(
                src_ref=sharesend.at[d - 1, c],
                dst_ref=sharerecv.at[d - 1, c],
                send_sem=osend_sem.at[d - 1, c],
                recv_sem=orecv_sem.at[d - 1, c],
                device_id=(me, target),
                device_id_type=MESH,
            )
            cp.start()
            sends.append(cp)
    mine = pl.ds(pl.multiple_of(core * rows, 16), rows)
    for c in range(chunks):
        total = jnp.dot(
            hidden[mine, :], wout[:, c * 512 : (c + 1) * 512], preferred_element_type=F32
        )
        for d in range(1, tp):
            sends[(d - 1) * chunks + c].wait_recv()
            total = total + sharerecv[d - 1, c].astype(F32)
        out_ref[:, c * 512 : (c + 1) * 512] = total.astype(BF16)

    for cp in sends:
        cp.wait_send()

    def settle(d, c):
        target = lax.rem(me + d, sp)
        meta_copy(me, target, d).wait_send()
        piece_copy(me, target, d).wait_send()

        @pl.when(target > 0)
        def _():
            prefix_copy(me, target).wait_send()

        return c

    lax.fori_loop(1, sp, settle, 0)


def body(sp, tp, tokens, norm_gain, wq, wk, wv, wo, wi, wf, cq, ck, offset, hgain, wout):
    rows, model = tokens.shape
    seq_len = rows * tp
    heads = offset.shape[2]
    qk, vd = wq.shape[1], wv.shape[1]
    dqk, dv = qk // heads, vd // heads
    piece = qk // sp
    chunks = wout.shape[1] // 512
    streams = (2 * qk + 2 * vd + wout.shape[1]) // 512
    hbm = pl.BlockSpec(memory_space=pl.ANY)
    vmem = pl.BlockSpec(memory_space=pltpu.VMEM)
    smem = pl.BlockSpec(memory_space=pltpu.SMEM)
    dma = pltpu.SemaphoreType.DMA
    return pl.pallas_call(
        functools.partial(kernel, sp, tp),
        out_shape=jax.ShapeDtypeStruct((rows, wout.shape[1]), BF16),
        in_specs=[hbm, vmem, hbm, hbm, hbm, hbm, vmem, vmem, vmem, vmem, smem, vmem, hbm],
        out_specs=vmem,
        scratch_shapes=[
            pltpu.VMEM((HALO + seq_len, model), BF16),
            pltpu.VMEM((HALO + seq_len, model), BF16),
            pltpu.VMEM(wq.shape, BF16),
            pltpu.VMEM(wk.shape, BF16),
            pltpu.VMEM(wv.shape, BF16),
            pltpu.VMEM(wo.shape, BF16),
            pltpu.VMEM(wout.shape, BF16),
            pltpu.VMEM((HALO + seq_len, qk), F32),
            pltpu.VMEM((seq_len, qk), BF16),
            pltpu.VMEM((seq_len, qk), BF16),
            pltpu.VMEM((seq_len, vd), BF16),
            pltpu.VMEM((seq_len, vd), BF16),
            pltpu.VMEM((seq_len, vd), F32),
            pltpu.VMEM((heads, seq_len, 128), F32),
            pltpu.VMEM((seq_len, vd), BF16),
            pltpu.VMEM((sp, piece, dv), BF16),
            pltpu.VMEM((sp, piece, dv), BF16),
            pltpu.VMEM((3, heads, dqk), F32),
            pltpu.VMEM((sp, 3, heads, dqk), F32),
            pltpu.VMEM((sp, piece, dv), BF16),
            pltpu.VMEM((sp, piece, dv), BF16),
            pltpu.VMEM((tp - 1, chunks, rows, 512), BF16),
            pltpu.VMEM((tp - 1, chunks, rows, 512), BF16),
            dma((streams,)),
            dma,
            dma((tp,)),
            dma((tp,)),
            dma,
            dma,
            dma((sp,)),
            dma((sp,)),
            dma((sp,)),
            dma((sp,)),
            dma((sp,)),
            dma((sp,)),
            dma((tp - 1, chunks)),
            dma((tp - 1, chunks)),
        ],
        compiler_params=pltpu.CompilerParams(
            collective_id=0, has_side_effects=True, vmem_limit_bytes=60 * 1024 * 1024
        ),
    )(
        tokens,
        norm_gain.reshape(1, model),
        wq,
        wk,
        wv,
        wo,
        wi.T,
        wf.T,
        cq,
        ck,
        offset,
        hgain.reshape(1, hgain.shape[0]),
        wout,
    )


def solution(mesh):
    in_specs = (
        P(("sp", "tp"), None),
        P(),
        P(None, "tp"),
        P(None, "tp"),
        P(None, "tp"),
        P(None, "tp"),
        P(),
        P(),
        P(),
        P(),
        P(None, "sp", "tp"),
        P(),
        P("tp", None),
    )
    out_specs = P(("sp", "tp"), None)
    step = functools.partial(body, mesh.shape["sp"], mesh.shape["tp"])
    return jax.shard_map(step, mesh=mesh, in_specs=in_specs, out_specs=out_specs, check_vma=False)
```

time: 244 us -> 44.6 us (0.18)
  the two profiles are of different devices: /device:TPU:15 before, /device:TPU:25 now
where the time goes in v1:
time: 44.6 us; the launch traced here: 44.4 us
  Pallas kernels  41 us (92%)
  local copies, waits for them, and re-layouts  3.37 us (8%)
    pallas_call x1, Pallas kernels, body(): pl.pallas_call(functools.partial(kernel, sp, tp), out_shape=jax.ShapeDtyp...  41 us
    unnamed x2, local copies, waits for them, and re-layouts  3.37 us

profile of v1, /device:TPU:25, one launch (start us, length us, event | category | flops | bytes accessed | tf_op | source)
XLA Modules:
  0.0 44.4 jit_solution(6557291506209798295)
XLA Ops:
  0.0 1.3 %copy.14.offset_ref = f32[2,3,4]{2,1,0:T(4,128)} copy(f32[2,3,4]{2,0,1:T(2,128)} %param.23) | data formatting | bytes 192 | tf_op args[10]
  1.3 41.0 %shard_map.127 = bf16[192,2048]{1,0:T(8,128)(2,1)} custom-call(bf16[192,2048]{1,0:T(8,128)(2,1)} %tokens_hbm.1, f32[1,2048]{1,0:T(1,128)} %bitcast.6, bf16[2048,512]{1,0:T(8,128)(2,1)} %wq_hbm.1, bf16[2048,512]{1,0:T(8,128)(2,1)} %wk_hbm.1, bf16[2048,1024]{1,0:T(8,128)(2,1)} %wv_hbm.1, bf16[2048,1024]{1,0:T(8,128)(2,1)} %wo_hbm.1, bf16[8,2048]{1,0:T(8,128)(2,1)} %bitcast.4, ...), custom_call_target="tpu_custom_call" | custom-call | tf_op jit(solution)/shard_map/pallas_call | solution.py:531
  42.3 2.1 %copy.16 = bf16[192,2048]{1,0:T(8,128)(2,1)} copy(bf16[192,2048]{1,0:T(8,128)(2,1)} %shard_map.127) | data formatting | bytes 1572864

commit v2 on v1

v2 whole, which is shorter than its diff:
```python
import functools

import jax
import jax.numpy as jnp
from jax import lax
from jax.experimental import pallas as pl
from jax.experimental.pallas import tpu as pltpu
from jax.sharding import PartitionSpec as P

SPAN = 128
HALO = 16
EPS = 1e-06
EMPTY_LEVEL = -1e30
HIGHEST = lax.Precision.HIGHEST
MESH = pl.DeviceIdType.MESH
F32, BF16 = jnp.float32, jnp.bfloat16


def normalize(values, gain):
    widened = values.astype(F32)
    scaled = widened * lax.rsqrt(jnp.mean(widened * widened, axis=-1, keepdims=True) + EPS)
    return (scaled * gain).astype(BF16)


def dot_t(a, b):
    return lax.dot_general(a, b, (((1,), (1,)), ((), ())), preferred_element_type=F32)


def dot_tl(a, b):
    return lax.dot_general(a, b, (((0,), (0,)), ((), ())), preferred_element_type=F32)


def kernel(
    sp,
    tp,
    tokens_hbm,
    gain_hbm,
    wq_hbm,
    wk_hbm,
    wv_hbm,
    wo_hbm,
    wi_hbm,
    wf_hbm,
    cq_hbm,
    ck_hbm,
    offset_hbm,
    hgain_hbm,
    wout_hbm,
    out_ref,
    gain_ref,
    wi_ref,
    wf_ref,
    cq_ref,
    ck_ref,
    offset_ref,
    hgain_ref,
    ext_own,
    ext_oth,
    nor_own,
    nor_oth,
    wq,
    wk,
    wv,
    wo,
    wout,
    gcol,
    kpre,
    qpre,
    key,
    query,
    value,
    ogate,
    numer,
    cols,
    hidden,
    sbuf,
    rbuf,
    meta,
    mbuf,
    nmeta,
    nbuf,
    scales,
    pbuf,
    gbuf,
    sharesend,
    sharerecv,
    w_sem,
    t_sem,
    s_sem,
    tsend_sem,
    trecv_sem,
    hsend_sem,
    hrecv_sem,
    psend_sem,
    precv_sem,
    msend_sem,
    mrecv_sem,
    nsend_sem,
    nrecv_sem,
    gsend_sem,
    grecv_sem,
    osend_sem,
    orecv_sem,
):
    me = lax.axis_index("sp")
    core = lax.axis_index("tp")
    rows, model = tokens_hbm.shape
    seq_len = rows * tp
    blocks = seq_len // SPAN
    heads = offset_hbm.shape[2]
    dqk = wq.shape[1] // heads
    dv = wv.shape[1] // heads
    piece_rows = sbuf.shape[1]
    head_first = core * heads
    last = tp - 1

    barrier = pltpu.get_barrier_semaphore()

    def signal(to_sp, to_tp):
        pl.semaphore_signal(barrier, inc=1, device_id=(to_sp, to_tp), device_id_type=MESH)

    def greet(d, c):
        signal(lax.rem(me + d, sp), core)
        return c

    lax.fori_loop(1, sp, greet, 0)
    for d in range(1, tp):
        signal(me, lax.rem(core + d, tp))

    @pl.when(core == last)
    def _():
        for c in range(tp - 1):
            signal(lax.rem(me + 1, sp), c)

    @pl.when(core != last)
    def _():
        signal(lax.rem(me + sp - 1, sp), last)

    own_copy = pltpu.make_async_copy(tokens_hbm, ext_own, t_sem)
    own_copy.start()
    small = []
    for n, (src, dst) in enumerate(
        (
            (gain_hbm, gain_ref),
            (wi_hbm, wi_ref),
            (wf_hbm, wf_ref),
            (ck_hbm, ck_ref),
            (cq_hbm, cq_ref),
            (offset_hbm, offset_ref),
            (hgain_hbm, hgain_ref),
        )
    ):
        cp = pltpu.make_async_copy(src, dst, s_sem.at[n])
        cp.start()
        small.append(cp)
    streams = {}
    at = 0
    for name, hbm, vm in (
        ("v", wv_hbm, wv),
        ("k", wk_hbm, wk),
        ("q", wq_hbm, wq),
        ("o", wo_hbm, wo),
        ("out", wout_hbm, wout),
    ):
        streams[name] = []
        for c in range(0, hbm.shape[1], 512):
            cp = pltpu.make_async_copy(
                hbm.at[:, pl.ds(c, 512)], vm.at[:, pl.ds(c, 512)], w_sem.at[at]
            )
            cp.start()
            streams[name].append(cp)
            at += 1

    for cp in small:
        cp.wait()
    own_copy.wait()
    gain = gain_ref[...]
    nor_own[...] = normalize(ext_own[...], gain)
    own = pl.ds(pl.multiple_of(core * rows, 16), rows)
    gate_weights = jnp.concatenate(
        [
            wi_ref[...].astype(F32),
            wf_ref[...].astype(F32),
            jnp.zeros((128 - 2 * wi_ref.shape[0], model), F32),
        ],
        axis=0,
    ).astype(BF16)
    gcol[own, :] = dot_t(nor_own[...], gate_weights)

    pl.semaphore_wait(barrier, sp - 1 + tp - 1 + jnp.where(core == last, tp - 1, 1))

    def token_copy(d, target, source):
        return pltpu.make_async_remote_copy(
            src_ref=ext_own,
            dst_ref=ext_oth.at[d - 1, pl.ds(0, rows)],
            send_sem=tsend_sem.at[d - 1],
            recv_sem=trecv_sem.at[d - 1],
            device_id=(me, target),
            device_id_type=MESH,
        )

    def halo_copy(c):
        return pltpu.make_async_remote_copy(
            src_ref=ext_own.at[pl.ds(rows - HALO, HALO)],
            dst_ref=ext_oth.at[tp - 2, pl.ds(rows, HALO)],
            send_sem=hsend_sem.at[c],
            recv_sem=hrecv_sem,
            device_id=(lax.rem(me + 1, sp), c),
            device_id_type=MESH,
        )

    sends_halo = jnp.logical_and(core == last, me < sp - 1)

    @pl.when(sends_halo)
    def _():
        for c in range(tp):
            halo_copy(c).start()

    for d in range(1, tp):
        token_copy(d, lax.rem(core + d, tp), None).start()

    def project(w, lhs, n):
        return jnp.dot(lhs, w[:, n : n + 256], preferred_element_type=F32).astype(BF16)

    qk, vd = wq.shape[1], wv.shape[1]
    pre_own = pl.ds(pl.multiple_of(HALO + core * rows, 16), rows)

    for c, cp in enumerate(streams["v"]):
        cp.wait()
        for n in range(c * 512, c * 512 + 512, 256):
            value[own, n : n + 256] = project(wv, nor_own[...], n)
    for cp in streams["k"]:
        cp.wait()
    for n in range(0, qk, 256):
        kpre[pre_own, n : n + 256] = project(wk, nor_own[...], n).astype(F32)

    @pl.when(sends_halo)
    def _():
        for c in range(tp):
            halo_copy(c).wait_send()

    for d in range(1, tp):
        cp = token_copy(d, lax.rem(core + d, tp), None)
        cp.wait_send()
        cp.wait_recv()
    for d in range(1, tp):
        nor_oth[d - 1, pl.ds(0, rows), :] = normalize(ext_oth[d - 1, pl.ds(0, rows), :], gain)

    def place(d):
        return lax.rem(core + tp - d, tp) * rows

    for d in range(1, tp):
        gcol[pl.ds(pl.multiple_of(place(d), 16), rows), :] = dot_t(
            nor_oth[d - 1, pl.ds(0, rows), :], gate_weights
        )

    gates_all = jnp.concatenate(
        [gcol[b * SPAN : (b + 1) * SPAN, :].T for b in range(blocks)], axis=1
    )
    total_heads = wi_ref.shape[0]
    in_rows = gates_all[:heads]
    fo_rows = gates_all[total_heads : total_heads + heads]
    for c in range(1, tp):
        in_rows = jnp.where(core == c, gates_all[c * heads : (c + 1) * heads], in_rows)
        fo_rows = jnp.where(
            core == c,
            gates_all[total_heads + c * heads : total_heads + (c + 1) * heads],
            fo_rows,
        )
    head_id = lax.broadcasted_iota(jnp.int32, (heads, SPAN), 0)

    def offsets(kind, b):
        spread = jnp.zeros((heads, SPAN), F32)
        for h in range(heads):
            spread = jnp.where(head_id == h, offset_ref[kind, b : b + 1, h : h + 1], spread)
        return spread

    upper = (
        lax.broadcasted_iota(jnp.int32, (SPAN, SPAN), 0)
        <= lax.broadcasted_iota(jnp.int32, (SPAN, SPAN), 1)
    ).astype(F32)
    gate, cum, tot = [], [], []
    for b in range(blocks):
        part = slice(b * SPAN, (b + 1) * SPAN)
        gate.append(in_rows[:, part] + offsets(0, b))
        x = fo_rows[:, part] + offsets(1, b)
        lf = jnp.minimum(x, 0.0) - jnp.log1p(jnp.exp(-jnp.abs(x)))
        lf8 = jnp.concatenate([lf, jnp.zeros((8 - heads, SPAN), F32)], axis=0) if heads < 8 else lf
        c = jnp.dot(lf8, upper, precision=HIGHEST, preferred_element_type=F32)[:heads]
        cum.append(c)
        tot.append(c[:, SPAN - 1 :])
    base = [jnp.zeros((heads, 1), F32)]
    for b in range(blocks):
        base.append(base[-1] + tot[b])
    tail = [None] * blocks
    acc = jnp.zeros((heads, 1), F32)
    for b in reversed(range(blocks)):
        tail[b] = acc
        acc = acc + tot[b]
    wlog = [tail[b] + (tot[b] - cum[b]) + gate[b] for b in range(blocks)]
    level = jnp.max(wlog[0], axis=1, keepdims=True)
    for b in range(1, blocks):
        level = jnp.maximum(level, jnp.max(wlog[b], axis=1, keepdims=True))
    wrows = [jnp.exp(w - level) for w in wlog]
    stacked = [jnp.concatenate([cum[b], wrows[b]], axis=0).T for b in range(blocks)]

    def to_peer(src, dst, ssem, rsem, target):
        return pltpu.make_async_remote_copy(
            src_ref=src,
            dst_ref=dst,
            send_sem=ssem,
            recv_sem=rsem,
            device_id=(target, core),
            device_id_type=MESH,
        )

    def meta_copy(source, target):
        return to_peer(meta, mbuf.at[source], msend_sem.at[target], mrecv_sem.at[source], target)

    def norm_copy(source, target):
        return to_peer(nmeta, nbuf.at[source], nsend_sem.at[target], nrecv_sem.at[source], target)

    def piece_copy(source, target):
        return to_peer(
            sbuf.at[target], rbuf.at[source], psend_sem.at[target], precv_sem.at[source], target
        )

    def prefix_copy(source, target):
        return to_peer(
            pbuf.at[target], gbuf.at[source], gsend_sem.at[target], grecv_sem.at[source], target
        )

    meta[0] = jnp.broadcast_to(base[blocks], (heads, dqk))
    meta[1] = jnp.broadcast_to(level, (heads, dqk))

    for n in range(0, vd, 256):
        for d in range(1, tp):
            value[pl.ds(pl.multiple_of(place(d), 16), rows), n : n + 256] = project(
                wv, nor_oth[d - 1, pl.ds(0, rows), :], n
            )

    def send_meta(d, c):
        meta_copy(me, lax.rem(me + d, sp)).start()
        return c

    lax.fori_loop(1, sp, send_meta, 0)
    mbuf[me] = meta[...]

    @pl.when(me > 0)
    def _():
        halo_copy(core).wait_recv()

    @pl.when(me == 0)
    def _():
        ext_oth[tp - 2, pl.ds(rows, HALO), :] = jnp.zeros((HALO, model), BF16)

    nor_oth[tp - 2, pl.ds(rows, HALO), :] = normalize(ext_oth[tp - 2, pl.ds(rows, HALO), :], gain)

    def rest_of(pre, w, n):
        for d in range(1, tp):
            more = HALO if d == tp - 1 else 0
            got = project(w, nor_oth[d - 1, pl.ds(0, rows + more), :], n).astype(F32)
            pre[pl.ds(pl.multiple_of(HALO + place(d), 16), rows), n : n + 256] = got[:rows]
            if more:
                pre[pl.ds(0, HALO), n : n + 256] = got[rows:]

    def mix(pre, taps_ref, dest, scale, n):
        taps = taps_ref[:, pl.ds(pl.multiple_of(core * qk + n, 128), 128)].astype(F32)
        count = taps.shape[0]
        mixed = jnp.zeros((seq_len, 128), F32)
        for j in range(count):
            mixed = (
                mixed
                + taps[j : j + 1, :] * pre[pl.ds(HALO - count + 1 + j, seq_len), n : n + 128]
            )
        dest[:, n : n + 128] = (mixed * jax.nn.sigmoid(mixed) * scale).astype(BF16)

    per = sp // heads
    for h in range(heads):
        if (h * dqk) % 256 == 0:
            rest_of(kpre, wk, h * dqk)
        mix(kpre, ck_ref, key, dqk**-0.5, h * dqk)
        weighted = [
            stacked[b][:, heads + h : heads + h + 1]
            * key[b * SPAN : (b + 1) * SPAN, h * dqk : (h + 1) * dqk].astype(F32)
            for b in range(blocks)
        ]
        norm = jnp.sum(weighted[0], axis=0, keepdims=True)
        for b in range(1, blocks):
            norm = norm + jnp.sum(weighted[b], axis=0, keepdims=True)
        state = dot_tl(
            jnp.concatenate([w.astype(BF16) for w in weighted], axis=0),
            value[:, h * dv : (h + 1) * dv],
        )
        for p in range(per):
            sbuf[p * heads + h] = state[p * piece_rows : (p + 1) * piece_rows].astype(BF16)
        nmeta[h : h + 1, :] = norm
        for p in range(per):
            target = p * heads + h

            @pl.when(me != target)
            def _():
                piece_copy(me, target).start()

            @pl.when(me == target)
            def _():
                rbuf[target] = sbuf[target]

    def send_norm(d, c):
        norm_copy(me, lax.rem(me + d, sp)).start()
        return c

    lax.fori_loop(1, sp, send_norm, 0)
    nbuf[me] = nmeta[...]

    for cp in streams["q"]:
        cp.wait()
    for n in range(0, qk, 256):
        qpre[pre_own, n : n + 256] = project(wq, nor_own[...], n).astype(F32)
        rest_of(qpre, wq, n)
        for m in range(n, n + 256, 128):
            mix(qpre, cq_ref, query, 1.0, m)

    my_head = lax.rem(me, heads)
    small_id = lax.broadcasted_iota(jnp.int32, (heads, dqk), 0)

    def weigh(i, carry):
        lev, lev_in = carry
        j = i - 1

        @pl.when(j != me)
        def _():
            meta_copy(j, me).wait_recv()

        shifted = lev + mbuf[j, 0]
        new_lev = jnp.maximum(shifted, mbuf[j, 1])
        one, two = jnp.exp(shifted - new_lev), jnp.exp(mbuf[j, 1] - new_lev)
        scales[i, 0] = one
        scales[i, 1] = two
        return new_lev, jnp.where(i == me, new_lev, lev_in)

    empty = jnp.full((heads, dqk), EMPTY_LEVEL, F32)
    _, lev_in = lax.fori_loop(1, sp, weigh, (empty, empty))

    causal = lax.broadcasted_iota(jnp.int32, (SPAN, SPAN), 0) >= lax.broadcasted_iota(
        jnp.int32, (SPAN, SPAN), 1
    )

    def intra(h):
        for i in range(blocks):
            col = stacked[i][:, h : h + 1]
            logs = []
            top = None
            for j in range(i + 1):
                row = (gate[j][h : h + 1] - cum[j][h : h + 1]) + (
                    base[i][h : h + 1] - base[j][h : h + 1]
                )
                tile = col + row
                if j == i:
                    tile = jnp.where(causal, tile, -jnp.inf)
                logs.append(tile)
                t = jnp.max(tile, axis=1, keepdims=True)
                top = t if top is None else jnp.maximum(top, t)
            q = query[i * SPAN : (i + 1) * SPAN, h * dqk : (h + 1) * dqk]
            den = jnp.zeros((SPAN, 1), F32)
            num = jnp.zeros((SPAN, dv), F32)
            for j in range(i + 1):
                k = key[j * SPAN : (j + 1) * SPAN, h * dqk : (h + 1) * dqk]
                scores = dot_t(q, k) * jnp.exp(logs[j] - top)
                den = den + jnp.sum(scores, axis=1, keepdims=True)
                num = num + jnp.dot(
                    scores.astype(BF16),
                    value[j * SPAN : (j + 1) * SPAN, h * dv : (h + 1) * dv],
                    preferred_element_type=F32,
                )
            numer[i * SPAN : (i + 1) * SPAN, h * dv : (h + 1) * dv] = num
            cols[h, i * SPAN : (i + 1) * SPAN, 0:1] = den
            cols[h, i * SPAN : (i + 1) * SPAN, 1:2] = top

    for h in range(heads // 2):
        intra(h)

    def pick(x):
        r = jnp.sum(jnp.where(small_id == my_head, x, 0.0), axis=0, keepdims=True)
        return jnp.concatenate([r] * (dv // dqk), axis=1)

    def combine(i, piece):
        j = i - 1
        one, two = pick(scales[i, 0]), pick(scales[i, 1])

        @pl.when(j != me)
        def _():
            piece_copy(j, me).wait_recv()

        piece = one * piece + two * rbuf[j].astype(F32)
        pbuf[i] = piece.astype(BF16)

        @pl.when(i == me)
        def _():
            gbuf[me] = piece.astype(BF16)

        @pl.when(jnp.logical_and(i > 1, j != me))
        def _():
            prefix_copy(me, j).start()

        return piece

    lax.fori_loop(1, sp, combine, jnp.zeros((piece_rows, dv), F32))

    @pl.when(me != sp - 1)
    def _():
        prefix_copy(me, sp - 1).start()

    for h in range(heads // 2, heads):
        intra(h)

    for c, cp in enumerate(streams["o"]):
        cp.wait()
        for n in range(c * 512, c * 512 + 512, 256):
            ogate[own, n : n + 256] = project(wo, nor_own[...], n)
            for d in range(1, tp):
                ogate[pl.ds(pl.multiple_of(place(d), 16), rows), n : n + 256] = project(
                    wo, nor_oth[d - 1, pl.ds(0, rows), :], n
                )

    @pl.when(me != sp - 1)
    def _():
        meta_copy(sp - 1, me).wait_recv()
        piece_copy(sp - 1, me).wait_recv()

    def take_norm(d, c):
        norm_copy(lax.rem(me + d, sp), me).wait_recv()
        return c

    lax.fori_loop(1, sp, take_norm, 0)
    nor_in = lax.fori_loop(
        1,
        me + 1,
        lambda i, nor: scales[i, 0] * nor + scales[i, 1] * nbuf[i - 1],
        jnp.zeros((heads, dqk), F32),
    )

    @pl.when(me == 0)
    def _():
        gbuf[...] = jnp.zeros(gbuf.shape, BF16)

    for h in range(heads):
        for p in range(per):
            source = p * heads + h

            @pl.when(jnp.logical_and(me > 0, me != source))
            def _():
                prefix_copy(source, me).wait_recv()

        state = jnp.concatenate([gbuf[p * heads + h] for p in range(per)], axis=0)
        hgain = hgain_ref[:, pl.ds(pl.multiple_of((head_first + h) * dv, 128), dv)]
        for i in range(blocks):
            part = slice(i * SPAN, (i + 1) * SPAN)
            q = query[part, h * dqk : (h + 1) * dqk]
            carried = (stacked[i][:, h : h + 1] + base[i][h : h + 1]) + lev_in[h : h + 1, 0:1]
            den, own_top = cols[h, part, 0:1], cols[h, part, 1:2]
            top = jnp.maximum(own_top, carried)
            new, old = jnp.exp(own_top - top), jnp.exp(carried - top)
            from_norm = jnp.sum(q.astype(F32) * nor_in[h : h + 1], axis=1, keepdims=True)
            den = new * den + old * from_norm
            num = new * numer[part, h * dv : (h + 1) * dv] + old * jnp.dot(
                q, state, preferred_element_type=F32
            )
            cell = num / jnp.maximum(jnp.abs(den), jnp.exp(-top))
            cell = cell * lax.rsqrt(jnp.mean(cell * cell, axis=-1, keepdims=True) + EPS)
            hidden[part, h * dv : (h + 1) * dv] = (
                cell * hgain * jax.nn.sigmoid(ogate[part, h * dv : (h + 1) * dv].astype(F32))
            ).astype(BF16)

    sends = []
    chunks = len(streams["out"])
    for c, cp in enumerate(streams["out"]):
        cp.wait()
    for d in range(1, tp):
        target = lax.rem(core + d, tp)
        theirs = pl.ds(pl.multiple_of(target * rows, 16), rows)
        for c in range(chunks):
            sharesend[d - 1, c] = jnp.dot(
                hidden[theirs, :], wout[:, c * 512 : (c + 1) * 512], preferred_element_type=F32
            ).astype(BF16)
            cp = pltpu.make_async_remote_copy(
                src_ref=sharesend.at[d - 1, c],
                dst_ref=sharerecv.at[d - 1, c],
                send_sem=osend_sem.at[d - 1, c],
                recv_sem=orecv_sem.at[d - 1, c],
                device_id=(me, target),
                device_id_type=MESH,
            )
            cp.start()
            sends.append(cp)
    for c in range(chunks):
        total = jnp.dot(
            hidden[own, :], wout[:, c * 512 : (c + 1) * 512], preferred_element_type=F32
        )
        for d in range(1, tp):
            sends[(d - 1) * chunks + c].wait_recv()
            total = total + sharerecv[d - 1, c].astype(F32)
        out_ref[:, c * 512 : (c + 1) * 512] = total.astype(BF16)

    for cp in sends:
        cp.wait_send()

    def settle(d, c):
        target = lax.rem(me + d, sp)
        meta_copy(me, target).wait_send()
        norm_copy(me, target).wait_send()
        piece_copy(me, target).wait_send()

        @pl.when(target > 0)
        def _():
            prefix_copy(me, target).wait_send()

        return c

    lax.fori_loop(1, sp, settle, 0)


def body(sp, tp, tokens, norm_gain, wq, wk, wv, wo, wi, wf, cq, ck, offset, hgain, wout):
    rows, model = tokens.shape
    seq_len = rows * tp
    heads = offset.shape[2]
    qk, vd = wq.shape[1], wv.shape[1]
    dqk, dv = qk // heads, vd // heads
    piece = qk // sp
    chunks = wout.shape[1] // 512
    streams = (2 * qk + 2 * vd + wout.shape[1]) // 512
    hbm = pl.BlockSpec(memory_space=pl.ANY)
    vmem = pl.BlockSpec(memory_space=pltpu.VMEM)
    dma = pltpu.SemaphoreType.DMA
    return pl.pallas_call(
        functools.partial(kernel, sp, tp),
        out_shape=jax.ShapeDtypeStruct((rows, wout.shape[1]), BF16),
        in_specs=[hbm] * 13,
        out_specs=vmem,
        scratch_shapes=[
            pltpu.VMEM((1, model), F32),
            pltpu.VMEM((wi.shape[1], model), BF16),
            pltpu.VMEM((wf.shape[1], model), BF16),
            pltpu.VMEM(cq.shape, BF16),
            pltpu.VMEM(ck.shape, BF16),
            pltpu.VMEM(offset.shape, F32),
            pltpu.VMEM((1, hgain.shape[0]), F32),
            pltpu.VMEM((rows, model), BF16),
            pltpu.VMEM((tp - 1, rows + HALO, model), BF16),
            pltpu.VMEM((rows, model), BF16),
            pltpu.VMEM((tp - 1, rows + HALO, model), BF16),
            pltpu.VMEM(wq.shape, BF16),
            pltpu.VMEM(wk.shape, BF16),
            pltpu.VMEM(wv.shape, BF16),
            pltpu.VMEM(wo.shape, BF16),
            pltpu.VMEM(wout.shape, BF16),
            pltpu.VMEM((seq_len, 128), F32),
            pltpu.VMEM((HALO + seq_len, qk), F32),
            pltpu.VMEM((HALO + seq_len, qk), F32),
            pltpu.VMEM((seq_len, qk), BF16),
            pltpu.VMEM((seq_len, qk), BF16),
            pltpu.VMEM((seq_len, vd), BF16),
            pltpu.VMEM((seq_len, vd), BF16),
            pltpu.VMEM((seq_len, vd), F32),
            pltpu.VMEM((heads, seq_len, 128), F32),
            pltpu.VMEM((seq_len, vd), BF16),
            pltpu.VMEM((sp, piece, dv), BF16),
            pltpu.VMEM((sp, piece, dv), BF16),
            pltpu.VMEM((2, heads, dqk), F32),
            pltpu.VMEM((sp, 2, heads, dqk), F32),
            pltpu.VMEM((heads, dqk), F32),
            pltpu.VMEM((sp, heads, dqk), F32),
            pltpu.VMEM((sp, 2, heads, dqk), F32),
            pltpu.VMEM((sp, piece, dv), BF16),
            pltpu.VMEM((sp, piece, dv), BF16),
            pltpu.VMEM((tp - 1, chunks, rows, 512), BF16),
            pltpu.VMEM((tp - 1, chunks, rows, 512), BF16),
            dma((streams,)),
            dma,
            dma((7,)),
            dma((tp - 1,)),
            dma((tp - 1,)),
            dma((tp,)),
            dma,
        ]
        + [dma((sp,))] * 8
        + [dma((tp - 1, chunks))] * 2,
        compiler_params=pltpu.CompilerParams(
            collective_id=0, has_side_effects=True, vmem_limit_bytes=60 * 1024 * 1024
        ),
    )(
        tokens,
        norm_gain.reshape(1, model),
        wq,
        wk,
        wv,
        wo,
        wi.T,
        wf.T,
        cq,
        ck,
        offset,
        hgain.reshape(1, hgain.shape[0]),
        wout,
    )


def solution(mesh):
    in_specs = (
        P(("sp", "tp"), None),
        P(),
        P(None, "tp"),
        P(None, "tp"),
        P(None, "tp"),
        P(None, "tp"),
        P(),
        P(),
        P(),
        P(),
        P(None, "sp", "tp"),
        P(),
        P("tp", None),
    )
    out_specs = P(("sp", "tp"), None)
    step = functools.partial(body, mesh.shape["sp"], mesh.shape["tp"])
    return jax.shard_map(step, mesh=mesh, in_specs=in_specs, out_specs=out_specs, check_vma=False)
```

time: 44.6 us -> 41 us (0.919)
  the two profiles are of different devices: /device:TPU:25 before, /device:TPU:15 now
where the time goes in v2:
time: 41 us; the launch traced here: 40.8 us
  Pallas kernels  37.4 us (91%)
  local copies, waits for them, and re-layouts  3.37 us (8%)
    pallas_call x1, Pallas kernels, body(): pl.pallas_call(functools.partial(kernel, sp, tp), out_shape=jax.ShapeDtyp...  37.4 us
    unnamed x2, local copies, waits for them, and re-layouts  3.37 us

profile of v2, /device:TPU:15, one launch (start us, length us, event | category | flops | bytes accessed | tf_op | source)
XLA Modules:
  0.0 40.8 jit_solution(1851296403795438864)
XLA Ops:
  0.0 1.3 %copy.14.offset_hbm = f32[2,3,4]{2,1,0:T(4,128)} copy(f32[2,3,4]{2,0,1:T(2,128)} %param.23) | data formatting | bytes 192 | tf_op args[10]
  1.3 37.4 %shard_map.127 = bf16[192,2048]{1,0:T(8,128)(2,1)} custom-call(bf16[192,2048]{1,0:T(8,128)(2,1)} %tokens_hbm.1, f32[1,2048]{1,0:T(1,128)} %bitcast.6, bf16[2048,512]{1,0:T(8,128)(2,1)} %wq_hbm.1, bf16[2048,512]{1,0:T(8,128)(2,1)} %wk_hbm.1, bf16[2048,1024]{1,0:T(8,128)(2,1)} %wv_hbm.1, bf16[2048,1024]{1,0:T(8,128)(2,1)} %wo_hbm.1, bf16[8,2048]{1,0:T(8,128)(2,1)} %bitcast.4, ...), custom_call_target="tpu_custom_call" | custom-call | tf_op jit(solution)/shard_map/pallas_call | solution.py:635
  38.7 2.1 %copy.16 = bf16[192,2048]{1,0:T(8,128)(2,1)} copy(bf16[192,2048]{1,0:T(8,128)(2,1)} %shard_map.127) | data formatting | bytes 1572864

commit v3 on v2

--- a/solution.py
+++ b/solution.py
@@ -272,7 +272,7 @@
     def offsets(kind, b):
         spread = jnp.zeros((heads, SPAN), F32)
         for h in range(heads):
-            spread = jnp.where(head_id == h, offset_ref[kind, b : b + 1, h : h + 1], spread)
+            spread = jnp.where(head_id == h, offset_ref[b, kind : kind + 1, h : h + 1], spread)
         return spread
 
     upper = (
@@ -629,12 +629,12 @@
     piece = qk // sp
     chunks = wout.shape[1] // 512
     streams = (2 * qk + 2 * vd + wout.shape[1]) // 512
-    hbm = pl.BlockSpec(memory_space=pl.ANY)
+    hbm = pl.BlockSpec(memory_space=pltpu.HBM)
     vmem = pl.BlockSpec(memory_space=pltpu.VMEM)
     dma = pltpu.SemaphoreType.DMA
     return pl.pallas_call(
         functools.partial(kernel, sp, tp),
-        out_shape=jax.ShapeDtypeStruct((rows, wout.shape[1]), BF16),
+        out_shape=pltpu.VMEM((rows, wout.shape[1]), BF16),
         in_specs=[hbm] * 13,
         out_specs=vmem,
         scratch_shapes=[
@@ -643,7 +643,7 @@
             pltpu.VMEM((wf.shape[1], model), BF16),
             pltpu.VMEM(cq.shape, BF16),
             pltpu.VMEM(ck.shape, BF16),
-            pltpu.VMEM(offset.shape, F32),
+            pltpu.VMEM((offset.shape[1], offset.shape[0], heads), F32),
             pltpu.VMEM((1, hgain.shape[0]), F32),
             pltpu.VMEM((rows, model), BF16),
             pltpu.VMEM((tp - 1, rows + HALO, model), BF16),
@@ -699,7 +699,7 @@
         wf.T,
         cq,
         ck,
-        offset,
+        jnp.transpose(offset, (1, 0, 2)),
         hgain.reshape(1, hgain.shape[0]),
         wout,
     )

time: 41 us -> 37.6 us (0.917)
  local copies, waits for them, and re-layouts: 3.37 us -> 0.88 us
  Pallas kernels: 37.4 us -> 36.5 us
    unnamed x2 -> x1, local copies, waits for them, and re-layouts: 3.37 us -> 0.88 us
    pallas_call x1, Pallas kernels: 37.4 us -> 36.5 us  [body(): pl.pallas_call(functools.partial(kernel, sp, tp), out_shape=pltpu.VMEM((r...]
where the time goes in v3:
time: 37.6 us; the launch traced here: 37.4 us
  Pallas kernels  36.5 us (97%)
  local copies, waits for them, and re-layouts  0.88 us (2%)
    pallas_call x1, Pallas kernels, body(): pl.pallas_call(functools.partial(kernel, sp, tp), out_shape=pltpu.VMEM((r...  36.5 us
    unnamed x1, local copies, waits for them, and re-layouts  0.88 us

profile of v3, /device:TPU:15, one launch (start us, length us, event | category | flops | bytes accessed | tf_op | source)
XLA Modules:
  0.0 37.4 jit_solution(5458047736540966377)
XLA Ops:
  0.0 36.5 %shard_map.127 = bf16[192,2048]{1,0:T(8,128)(2,1)S(1)} custom-call(bf16[192,2048]{1,0:T(8,128)(2,1)} %tokens_hbm.1, f32[1,2048]{1,0:T(1,128)} %bitcast.7, bf16[2048,512]{1,0:T(8,128)(2,1)} %wq_hbm.1, bf16[2048,512]{1,0:T(8,128)(2,1)} %wk_hbm.1, bf16[2048,1024]{1,0:T(8,128)(2,1)} %wv_hbm.1, bf16[2048,1024]{1,0:T(8,128)(2,1)} %wo_hbm.1, ...), custom_call_target="tpu_custom_call" | custom-call | tf_op jit(solution)/shard_map/pallas_call | solution.py:635
  36.6 0.9 %copy.15 = bf16[192,2048]{1,0:T(8,128)(2,1)} copy(bf16[192,2048]{1,0:T(8,128)(2,1)S(1)} %shard_map.127) | data formatting | bytes 1572864
